TPU v7x, 512 devices: a 4x2x32 block of a 4x8x32 slice. The times are simulated.
512 devices in a mesh: grp: 2 (over y), fs: 32 (over z), tp: 8 (over x, core).
Axes of the slice: x: 4, y: 2, z: 32, core: 2. Of those that a mesh axis runs over, the one named last changes fastest.
The devices are a block of a 4x8x32 slice.
Arguments:
- stream: bfloat16 [2048, 24576], P('tp', ('grp', 'fs')), parts along dimension 1, may hold values from -6 to 6
- mixer_gain: float32 [2048], replicated, may hold values from 0.1 to 1.9
- glu_value: bfloat16 [2048, 1024], P('fs', 'tp'), may hold values from -0.125 to 0.125
- glu_gate: bfloat16 [2048, 1024], P('fs', 'tp'), may hold values from -0.125 to 0.125
- conv_kernel: bfloat16 [31, 1024], replicated, may hold values from -1 to 1
- channel_gain: float32 [1024], replicated, may hold values from 0.1 to 1.9
- conv_out: bfloat16 [2048, 1024], P('fs', 'tp'), may hold values from -0.1875 to 0.1875
- ffn_gain: float32 [2048], replicated, may hold values from 0.1 to 1.9
- ffn_gate: bfloat16 [2048, 5632], P('fs', 'tp'), may hold values from -0.125 to 0.125
- ffn_up: bfloat16 [2048, 5632], P('fs', 'tp'), may hold values from -0.125 to 0.125
- ffn_down: bfloat16 [2048, 5632], P('fs', 'tp'), may hold values from -0.078125 to 0.078125
Outputs:
- result: bfloat16 [2048, 24576], P('tp', ('grp', 'fs')), parts along dimension 1
There are 2 independent parts, one for each index of `grp`. A program takes and returns all parts, laid end to end along the dimension named above; an argument that names none is the same for every part. Nothing has to cross between parts.
All inputs are finite; a program needn't handle non-finite values.
Results may differ from a plain program's by a relative error of at most 0.018.
Values may be sent and summed in bfloat16 or wider, within the bound.
A program may use at most 64 MiB of HBM per device.

v0:
```python
import jax
import jax.numpy as jnp
from jax import lax
from jax.sharding import PartitionSpec as P


def in_order(parts, dim):
    parts = jnp.moveaxis(parts, 0, dim)
    shape = parts.shape
    return parts.reshape(*shape[:dim], shape[dim] * shape[dim + 1], *shape[dim + 2 :])


def copy_for_each(value, axis):
    peers = lax.axis_size(axis)
    return lax.all_to_all(
        jnp.broadcast_to(value[None], (peers, *value.shape)), axis, 0, 0, tiled=True
    )


def gather_directly(value, axis, dim):
    return in_order(copy_for_each(value, axis), dim)


def sent_together(arrays, axis, dim, along):
    widths = [a.shape[along] for a in arrays]
    both = jnp.concatenate(arrays, axis=along)
    out = lax.all_gather(both, axis, axis=dim, tiled=True)
    return tuple(jnp.split(out, [sum(widths[:k]) for k in range(1, len(widths))], axis=along))


def over_copies(value, axis):
    everything = copy_for_each(value, axis)
    return jnp.sum(everything, axis=0)


def together(arrays, axis):
    ends = [0]
    for a in arrays:
        ends.append(ends[-1] + a.size)
    so_far = over_copies(jnp.concatenate([a.ravel() for a in arrays]), axis)
    return tuple((so_far[b:e].reshape(a.shape) for a, b, e in zip(arrays, ends, ends[1:])))


def cut_along(value, dim, peers):
    shape = value.shape
    parts = value.reshape(*shape[:dim], peers, shape[dim] // peers, *shape[dim + 1 :])
    return jnp.moveaxis(parts, dim, 0)


def sent_and_summed(value, axis, dim):
    parts = cut_along(value, dim, lax.axis_size(axis))
    arrived = lax.all_to_all(parts, axis, split_axis=0, concat_axis=0, tiled=True)
    return arrived.astype(jnp.float32).sum(axis=0)


def rms_normalize(wide, gain):
    inverse = lax.rsqrt(jnp.mean(wide * wide, axis=0, keepdims=True) + 1e-06)
    return (wide * inverse * gain[:, None]).astype(jnp.bfloat16)


def contract(weight, acts):
    return lax.dot_general(
        weight, acts, (((0,), (0,)), ((), ())), preferred_element_type=jnp.float32
    )


def on_device(
    stream,
    mixer_gain,
    glu_value,
    glu_gate,
    conv_kernel,
    channel_gain,
    conv_out,
    ffn_gain,
    ffn_gate,
    ffn_up,
    ffn_down,
):
    length = stream.shape[1]
    channels = glu_value.shape[1]
    position = lax.axis_index("tp")
    total_channels = channels * lax.axis_size("tp")
    taps = lax.dynamic_slice_in_dim(conv_kernel, position * channels, channels, 1).astype(
        jnp.float32
    )
    gain_local = lax.dynamic_slice_in_dim(channel_gain, position * channels, channels, 0)
    gathered = gather_directly(stream, "tp", 0)
    normed = rms_normalize(gathered.astype(jnp.float32), mixer_gain)
    value_w, gate_w, out_w = sent_together((glu_value, glu_gate, conv_out), "fs", 0, 1)
    value_part = contract(value_w, normed)
    gate_part = contract(gate_w, normed)
    gated = (value_part * jax.nn.sigmoid(gate_part)).astype(jnp.bfloat16).astype(jnp.float32)
    padded = jnp.pad(gated, ((0, 0), (taps.shape[0] - 1, 0)))
    conv_sum = jnp.zeros_like(gated)
    for step in range(taps.shape[0]):
        conv_sum = conv_sum + taps[step][:, None] * padded[:, step : step + length]
    sums, squares = together(
        (jnp.sum(conv_sum, axis=0), jnp.sum(conv_sum * conv_sum, axis=0)), "tp"
    )
    mean_val = sums / total_channels
    mean_sq = squares / total_channels
    scaled = (
        (conv_sum - mean_val[None, :])
        * lax.rsqrt(mean_sq - mean_val * mean_val + 1e-05)[None, :]
        * gain_local[:, None]
    )
    activated = jax.nn.silu(scaled).astype(jnp.bfloat16)
    mixed_sum = sent_and_summed(
        jnp.dot(out_w, activated, preferred_element_type=jnp.float32).astype(jnp.bfloat16), "tp", 0
    )
    middle_wide = stream.astype(jnp.float32) + mixed_sum
    middle = middle_wide.astype(jnp.bfloat16)
    gathered_two = gather_directly(middle, "tp", 0)
    normed_two = rms_normalize(gathered_two.astype(jnp.float32), ffn_gain)
    gate_whole, up_whole = sent_together((ffn_gate, ffn_up), "fs", 0, 1)
    gate_val = contract(gate_whole, normed_two)
    up_val = contract(up_whole, normed_two)
    hidden = (jax.nn.silu(gate_val) * up_val).astype(jnp.bfloat16)
    down_whole = lax.all_gather(ffn_down, "fs", axis=0, tiled=True)
    ffn_sum = sent_and_summed(
        jnp.dot(down_whole, hidden, preferred_element_type=jnp.float32).astype(jnp.bfloat16),
        "tp",
        0,
    )
    return (middle.astype(jnp.float32) + ffn_sum).astype(jnp.bfloat16)


def solution(mesh):
    in_specs = (
        P("tp", ("grp", "fs")),
        P(),
        P("fs", "tp"),
        P("fs", "tp"),
        P(),
        P(),
        P("fs", "tp"),
        P(),
        P("fs", "tp"),
        P("fs", "tp"),
        P("fs", "tp"),
    )
    out_specs = P("tp", ("grp", "fs"))
    return jax.shard_map(
        on_device, mesh=mesh, in_specs=in_specs, out_specs=out_specs, check_vma=False
    )
```

profile of v0, /device:TPU:33, one launch (start us, length us, event | category | flops | bytes accessed | tf_op | source)
XLA Modules:
  0.0 480.1 jit_solution(7017080481683347827)
XLA Ops:
  6.6 1.4 pad_maximum_fusion.1
  8.1 1.7 pad_maximum_fusion
  9.8 2.2 broadcast_in_dim.6
  12.1 44.9 %all-to-all-start = ((bf16[8,256,384]{2,1,0:T(8,128)(2,1)}), bf16[8,256,384]{2,1,0:T(8,128)(2,1)S(1)}, u32[]{:S(2)}, u32[]{:S(2)}) async-start(bf16[8,256,384]{2,1,0:T(8,128)(2,1)} %broadcast_in_dim.6), calls=%async_computation | async-start | bytes 3145728 | tf_op jit(solution)/shard_map/all_to_all | solution.py:15
  57.0 0.7 all-gather.8.cloned.1.call-update
  57.7 0.7 dynamic-slice_convert_fusion
  58.5 19.2 %all-to-all-done = bf16[8,256,384]{2,1,0:T(8,128)(2,1)S(1)} async-done(((bf16[8,256,384]{2,1,0:T(8,128)(2,1)}), bf16[8,256,384]{2,1,0:T(8,128)(2,1)S(1)}, u32[]{:S(2)}, u32[]{:S(2)}) %all-to-all-start) | async-done | bytes 1572896 | tf_op jit(solution)/shard_map/all_to_all | solution.py:15
  77.7 0.4 multiply_reduce_fusion.1
  78.1 0.4 fusion.7
  78.5 71.5 %all-gather.4.cloned.1.call-done = bf16[2048,384]{1,0:T(8,128)(2,1)} async-done(((bf16[64,384]{1,0:T(8,128)(2,1)}), bf16[2048,384]{1,0:T(8,128)(2,1)}) %all-gather.4.cloned.1.call-update) | async-done | bytes 1572880 | tf_op jit(solution)/shard_map/all_gather | solution.py:27
  150.1 1.5 fusion.24
  151.6 1.5 fusion.19
  153.1 2.3 fusion.93
  155.5 0.6 broadcast_in_dim.7
  156.1 25.3 %all-to-all-start.1 = ((f32[8,1,768]{2,1,0:T(1,128)}), f32[8,1,768]{2,1,0:T(1,128)S(1)}, u32[]{:S(2)}, u32[]{:S(2)}) async-start(f32[8,1,768]{2,1,0:T(1,128)} %broadcast_in_dim.7), calls=%async_computation.1 | async-start | bytes 49152 | tf_op jit(solution)/shard_map/all_to_all | solution.py:15
  181.4 0.8 dynamic_slice.7
  182.2 3.9 all-to-all-done.1
  186.2 1.7 convolution_convert_fusion.1
  187.9 23.8 %all_to_all.26 = bf16[8,256,384]{2,1,0:T(8,128)(2,1)S(1)} all-to-all(bf16[8,256,384]{2,1,0:T(8,128)(2,1)S(1)} %bitcast.85), channel_id=1, replica_groups=mesh['grp'=2,'fs'=32,'tp'=8] {'tp'}, dimensions={0} | all-to-all | bytes 3145728 | tf_op jit(solution)/shard_map/all_to_all | solution.py:52
  211.7 0.2 convert_reduce_fusion.1
  211.9 0.7 copy-done
  212.8 24.1 %all_to_all.27 = bf16[8,256,384]{2,1,0:T(8,128)(2,1)S(1)} all-to-all(bf16[8,256,384]{2,1,0:T(8,128)(2,1)S(1)} %broadcast_in_dim.8), channel_id=1, replica_groups=mesh['grp'=2,'fs'=32,'tp'=8] {'tp'}, dimensions={0} | all-to-all | bytes 3145728 | tf_op jit(solution)/shard_map/all_to_all | solution.py:15
  236.9 0.4 multiply_reduce_fusion
  237.3 0.3 copy-done.2
  237.6 0.4 fusion.5
  238.0 51.1 %all-gather.6.cloned.1.call-done = bf16[2048,1408]{1,0:T(8,128)(2,1)} async-done(((bf16[64,1408]{1,0:T(8,128)(2,1)}), bf16[2048,1408]{1,0:T(8,128)(2,1)}) %all-gather.6.cloned.1.call-update) | async-done | bytes 5767184 | tf_op jit(solution)/shard_map/all_gather | solution.py:27
  289.1 4.6 fusion.2
  293.8 126.2 %all-gather.8.cloned.1.call-done = bf16[2048,704]{1,0:T(8,128)(2,1)} async-done(((bf16[64,704]{1,0:T(8,128)(2,1)}), bf16[2048,704]{1,0:T(8,128)(2,1)}) %all-gather.8.cloned.1.call-update) | async-done | bytes 2883600 | tf_op jit(solution)/shard_map/all_gather | solution.py:120
  419.9 6.9 %convolution_convert_fusion = bf16[384,2048]{1,0:T(8,128)(2,1)S(1)} fusion(bf16[2048,704]{1,0:T(8,128)(2,1)} %all-gather.8.cloned.1.call-done, bf16[2048,384]{1,0:T(8,128)(2,1)S(1)} %fusion.5, bf16[2048,1408]{1,0:T(8,128)(2,1)} %all-gather.6.cloned.1.call-done, f32[704,384]{1,0:T(8,128)} %fusion.2), kind=kOutput, calls=%fused_computation.14 | convolution fusion | flops 2217000960 | bytes 10518528 | tf_op jit(solution)/shard_map/dot_general | solution.py:122
  426.9 45.5 %all_to_all.28 = bf16[8,256,384]{1,2,0:T(8,128)(2,1)S(1)} all-to-all(bf16[8,256,384]{1,2,0:T(8,128)(2,1)S(1)} %bitcast.86), channel_id=1, replica_groups=mesh['grp'=2,'fs'=32,'tp'=8] {'tp'}, dimensions={0} | all-to-all | bytes 3145728 | tf_op jit(solution)/shard_map/all_to_all | solution.py:52
  472.5 0.2 convert_reduce_fusion
  472.9 0.7 add_convert_fusion
  (20 shorter events, 0.7 us)
Async XLA Ops:
  6.5 143.5 %all-gather.4.cloned.1.call-start = ((), (), s32[]{:S(2)}) async-start(), calls=%async_computation.5 | async-start | bytes 1622016 | tf_op jit(solution)/shard_map/all_gather | solution.py:27
  8.0 281.2 %all-gather.6.cloned.1.call-start = ((), (), s32[]{:S(2)}) async-start(), calls=%async_computation.6 | async-start | bytes 5947392 | tf_op jit(solution)/shard_map/all_gather | solution.py:27
  12.1 65.6 %all-to-all-start = ((bf16[8,256,384]{2,1,0:T(8,128)(2,1)}), bf16[8,256,384]{2,1,0:T(8,128)(2,1)S(1)}, u32[]{:S(2)}, u32[]{:S(2)}) async-start(bf16[8,256,384]{2,1,0:T(8,128)(2,1)} %broadcast_in_dim.6), calls=%async_computation | async-start | bytes 3145728 | tf_op jit(solution)/shard_map/all_to_all | solution.py:15
  57.0 21.1 %copy-start.1 = (f32[2048]{0:T(1024)S(1)}, f32[2048]{0:T(1024)}, u32[]{:S(2)}) copy-start(f32[2048]{0:T(1024)} %param.12) | copy-start | bytes 24580
  57.0 363.0 %all-gather.8.cloned.1.call-start = ((), (), s32[]{:S(2)}) async-start(), calls=%async_computation.7 | async-start | bytes 3244032 | tf_op jit(solution)/shard_map/all_gather | solution.py:120
  156.1 30.0 %all-to-all-start.1 = ((f32[8,1,768]{2,1,0:T(1,128)}), f32[8,1,768]{2,1,0:T(1,128)S(1)}, u32[]{:S(2)}, u32[]{:S(2)}) async-start(f32[8,1,768]{2,1,0:T(1,128)} %broadcast_in_dim.7), calls=%async_computation.1 | async-start | bytes 49152 | tf_op jit(solution)/shard_map/all_to_all | solution.py:15
  211.7 0.9 copy-start
  236.9 0.7 copy-start.2
Sparse Core Ops, SparseCore 0:
  9.4 140.5 all-gather.3
  152.1 136.9 all-gather.5
  291.2 128.6 all-gather.7
where the time goes:
time: 481 us; the launch traced here: 480 us
  waiting for transfers between devices  273 us (57%)
  blocking collectives  93.4 us (19%)
  starting transfers between devices  70.3 us (15%)
  matrix products  16.3 us (3%)
  between operations  13.2 us (3%)
  other arithmetic  9.04 us (2%)
  local copies, waits for them, and re-layouts  5 us (1%)
    all_gather x1, waiting for transfers between devices, on_device(): down_whole = lax.all_gather(ffn_down, 'fs', axis=0, tiled=True)  126 us
    all_gather x2, waiting for transfers between devices, sent_together(): out = lax.all_gather(both, axis, axis=dim, tiled=True)  123 us
    all_to_all x2, starting transfers between devices, copy_for_each(): lax.all_to_all(jnp.broadcast_to(value[None], (peers, *value.shape)), axis...  70.3 us
    all_to_all x2, blocking collectives, sent_and_summed(): lax.all_to_all(parts, axis, split_axis=0, concat_axis=0, tiled=True)  69.4 us
    all_to_all x1, blocking collectives, copy_for_each(): lax.all_to_all(jnp.broadcast_to(value[None], (peers, *value.shape)), axis...  24.1 us
    all_to_all x2, waiting for transfers between devices, copy_for_each(): lax.all_to_all(jnp.broadcast_to(value[None], (peers, *value.shape)), axis...  23.1 us
  transfers between devices with their start and end apart: 5, of which 5 were waited for; matrix products, arithmetic and copies ran while one was open for 4% of the time, Pallas kernels for 0%

commit v1 on v0

v1 whole, which is shorter than its diff:
```python
import functools

import jax
import jax.numpy as jnp
from jax import lax
from jax.experimental import pallas as pl
from jax.experimental.pallas import tpu as pltpu
from jax.sharding import PartitionSpec as P

MESH = pl.DeviceIdType.MESH
BF, F32 = jnp.bfloat16, jnp.float32
CW, CCW = 0, 1


def dot_nn(a, b):
    return lax.dot_general(a, b, (((1,), (0,)), ((), ())), preferred_element_type=F32)


def dot_nt(a, b):
    return lax.dot_general(a, b, (((1,), (1,)), ((), ())), preferred_element_type=F32)


def kernel(
    nz, nt,
    stream, mixer_gain, conv_kernel, channel_gain, ffn_gain, gv, gg, co, wg, wu, wd,
    out,
    glu, gu, dn, ag1, ag2, nrm, pad, cvt, act, stats, hid, acc, mid,
    pb, rb, sb, cb, pb2, rb2, sb2, cb2,
    loc_sem, zsend, zrecv, ysend, yrecv, ag_send, ag_recv, st_send, st_recv,
    d_send, d_recv, c_send, c_recv,
):
    g, z, t = lax.axis_index("grp"), lax.axis_index("fs"), lax.axis_index("tp")
    gi = lax.rem(g, 2)
    mate = g + 1 - 2 * gi
    core = lax.rem(t, 2)
    x = t // 2
    nx = nt // 2
    twin = t + 1 - 2 * core
    right, left = lax.rem(z + 1, nz), lax.rem(z + nz - 1, nz)
    rows, toks = stream.shape
    width = rows * nt
    srows = gv.shape[0]
    chans = gv.shape[1]
    taps = conv_kernel.shape[0]
    ncw, nccw = nz // 2, nz - 1 - nz // 2

    def at_chip(o):
        return lax.rem(x + o, nx) * 2 + core

    own = pl.ds(pl.multiple_of(z * srows, srows), srows)
    locals_ = [
        pltpu.make_async_copy(gv, glu.at[own, pl.ds(0, chans)], loc_sem.at[0]),
        pltpu.make_async_copy(gg, glu.at[own, pl.ds(chans, chans)], loc_sem.at[1]),
        pltpu.make_async_copy(co, glu.at[own, pl.ds(2 * chans, chans)], loc_sem.at[2]),
        pltpu.make_async_copy(wg, gu.at[0, own, :], loc_sem.at[3]),
        pltpu.make_async_copy(wu, gu.at[1, own, :], loc_sem.at[4]),
        pltpu.make_async_copy(wd, dn.at[own, :], loc_sem.at[5]),
    ]
    for c in locals_:
        c.start()

    barrier = pltpu.get_barrier_semaphore()
    for peer in (right, left):
        pl.semaphore_signal(barrier, inc=1, device_id={"fs": peer}, device_id_type=MESH)
    pl.semaphore_signal(barrier, inc=1, device_id={"grp": mate}, device_id_type=MESH)
    for o in range(1, nt):
        pl.semaphore_signal(
            barrier, inc=1, device_id={"tp": lax.rem(t + o, nt)}, device_id_type=MESH
        )
    ag1[t] = stream[...].T
    for c in locals_:
        c.wait()
    pl.semaphore_wait(barrier, 2 + nt)

    half, quarter = srows // 2, srows // 4

    def slot(p, zz):
        base = zz * srows
        if p < 2:
            return glu.at[pl.ds(pl.multiple_of(base + half * p, half), half), :]
        k = (p - 2) % 4
        r = pl.ds(pl.multiple_of(base + quarter * k, quarter), quarter)
        return gu.at[gi, r, :] if p < 6 else dn.at[r, :]

    def zcopy(p, d, zz, s):
        return pltpu.make_async_remote_copy(
            src_ref=slot(p, zz), dst_ref=slot(p, zz),
            send_sem=zsend.at[d, p], recv_sem=zrecv.at[d, p, s - 1],
            device_id={"fs": right if d == CW else left}, device_id_type=MESH,
        )

    def held(d, s):
        return lax.rem(z - s + nz, nz) if d == CW else lax.rem(z + s, nz)

    def send(p, d, s):
        zcopy(p, d, held(d, s - 1), s).start()

    def ycopy(d, s, whose):
        r = pl.ds(pl.multiple_of(held(d, s) * srows, srows), srows)
        i = d * ncw + s - 1
        return pltpu.make_async_remote_copy(
            src_ref=gu.at[whose, r, :], dst_ref=gu.at[whose, r, :],
            send_sem=ysend, recv_sem=yrecv.at[i],
            device_id={"grp": mate}, device_id_type=MESH,
        )

    def step(pieces, s, dirs, fwd):
        for p in pieces:
            for d in dirs:
                zcopy(p, d, held(d, s), s).wait_recv()
                if d in fwd:
                    send(p, d, s + 1)
        if 5 in pieces:
            for d in dirs:
                ycopy(d, s, gi).start()

    def first(pieces):
        for p in pieces:
            for d in (CW, CCW):
                send(p, d, 1)

    def rounds(pieces, lo, hi):
        top = min(hi, nccw)
        if top > lo:
            @pl.loop(lo, top)
            def _(s):
                step(pieces, s, (CW, CCW), (CW, CCW))
        for s in range(max(lo, nccw), hi):
            step(
                pieces, s,
                (CW, CCW) if s <= nccw else (CW,),
                (CW,) if s < ncw else (),
            )

    def ag_copy(buf, which, block, k, target):
        return pltpu.make_async_remote_copy(
            src_ref=buf.at[block], dst_ref=buf.at[block],
            send_sem=ag_send.at[which, k], recv_sem=ag_recv.at[which, block],
            device_id={"tp": target}, device_id_type=MESH,
        )

    def ag_start(buf, which):
        for k, o in enumerate((2, 1, 3)):
            ag_copy(buf, which, t, k, at_chip(o)).start()
        ag_copy(buf, which, t, 3, twin).start()

    def ag_forward(buf, which, os):
        for o in os:
            b = at_chip(o)
            ag_copy(buf, which, b, 0, twin).wait_recv()
            ag_copy(buf, which, b, 3 + o, twin).start()

    def ag_finish(buf, which):
        ag_copy(buf, which, twin, 0, twin).wait_recv()
        for o in range(1, nx):
            ag_copy(buf, which, lax.rem(x + o, nx) * 2 + 1 - core, 0, twin).wait_recv()

    def ag_drain(buf, which):
        for k in range(4):
            ag_copy(buf, which, t, k, twin).wait_send()
        for o in range(1, nx):
            ag_copy(buf, which, at_chip(o), 3 + o, twin).wait_send()

    tb = toks // 3

    def normalize(buf, gain, b):
        r = pl.ds(b * tb, tb)
        total = jnp.zeros((tb, rows), F32)
        for j in range(nt):
            v = buf[j, r, :].astype(F32)
            total = total + v * v
        inv = lax.rsqrt(jnp.sum(total, axis=1, keepdims=True) / width + 1e-06)
        for j in range(nt):
            v = buf[j, r, :].astype(F32)
            nrm[r, j * rows:(j + 1) * rows] = (
                v * inv * gain[:, j * rows:(j + 1) * rows]
            ).astype(BF)

    order = (2, 1, 3, 0)

    def d_copy(which, o, pbuf, rbuf):
        return pltpu.make_async_remote_copy(
            src_ref=pbuf.at[o], dst_ref=rbuf.at[o],
            send_sem=d_send.at[which, o], recv_sem=d_recv.at[which, o],
            device_id={"tp": twin}, device_id_type=MESH,
        )

    def c_copy(which, o, sbuf, cbuf):
        return pltpu.make_async_remote_copy(
            src_ref=sbuf.at[o - 1], dst_ref=cbuf.at[o - 1],
            send_sem=c_send.at[which, o - 1], recv_sem=c_recv.at[which, o - 1],
            device_id={"tp": at_chip(o)}, device_id_type=MESH,
        )

    def rs_first(which, partial, pbuf, rbuf):
        for o in order:
            td = lax.rem(x + o, nx) * 2 + 1 - core
            pbuf[o] = partial(td).astype(BF)
            d_copy(which, o, pbuf, rbuf).start()

    def rs_second(which, partial, pbuf, rbuf, sbuf, cbuf):
        for o in order:
            mine = partial(at_chip(o))
            d_copy(which, o, pbuf, rbuf).wait_recv()
            both = mine + rbuf[o].astype(F32)
            if o:
                sbuf[o - 1] = both.astype(BF)
                c_copy(which, o, sbuf, cbuf).start()
            else:
                acc[...] = both

    def rs_third(which, sbuf, cbuf):
        total = acc[...]
        for o in order[:3]:
            c_copy(which, o, sbuf, cbuf).wait_recv()
            total = total + cbuf[o - 1].astype(F32)
        return total

    def rs_drain(which, pbuf, rbuf, sbuf, cbuf):
        for o in order:
            d_copy(which, o, pbuf, rbuf).wait_send()
            if o:
                c_copy(which, o, sbuf, cbuf).wait_send()

    def out_rows(td):
        return pl.ds(pl.multiple_of(td * rows, rows), rows)

    early = (0, 1, 2, 3, 4, 5)
    late = (6, 7, 8, 9)
    first((0, 1))
    ag_start(ag1, 0)
    first((2, 3, 4, 5))
    rounds(early, 1, 4)
    ag_forward(ag1, 0, (1, 3))
    rounds(early, 4, 5)
    ag_forward(ag1, 0, (2,))
    rounds(early, 5, 7)
    ag_finish(ag1, 0)
    normalize(ag1, mixer_gain, 0)
    rounds(early, 7, 8)
    normalize(ag1, mixer_gain, 1)
    rounds(early, 8, 9)
    normalize(ag1, mixer_gain, 2)
    pad[0:32, :] = jnp.zeros((32, chans), F32)
    rounds(early, 9, nz // 2)
    first(late)
    rounds(early, nz // 2, nz // 2 + 1)

    both = dot_nn(nrm[...], glu[:, 0:2 * chans])
    gated = both[:, :chans] * jax.nn.sigmoid(both[:, chans:])
    pad[32:32 + toks, :] = gated.astype(BF).astype(F32)
    rounds(late, 1, 2)
    lanes = pl.ds(pl.multiple_of(t * chans, chans), chans)
    kern = conv_kernel[:, lanes].astype(F32)
    nb = 6
    bt = toks // nb
    for b in range(nb):
        total = jnp.zeros((bt, chans), F32)
        for k in range(taps):
            lo = b * bt + 32 - (taps - 1) + k
            total = total + kern[k:k + 1, :] * pad[lo:lo + bt, :]
        cvt[b * bt:(b + 1) * bt, :] = total
    flipped = cvt[...].T
    stats[t, 0:1, :] = jnp.sum(flipped, axis=0, keepdims=True)
    stats[t, 1:2, :] = jnp.sum(flipped * flipped, axis=0, keepdims=True)

    def st_copy(o, src, target):
        return pltpu.make_async_remote_copy(
            src_ref=stats.at[src], dst_ref=stats.at[src],
            send_sem=st_send.at[o], recv_sem=st_recv.at[src],
            device_id={"tp": target}, device_id_type=MESH,
        )

    for o in range(1, nt):
        st_copy(o, t, lax.rem(t + o, nt)).start()
    rounds(late, 2, 3)
    for o in range(1, nt):
        st_copy(o, lax.rem(t + o, nt), lax.rem(t + o, nt)).wait_recv()
    total = stats[0]
    for j in range(1, nt):
        total = total + stats[j]
    total = total / (chans * nt)
    mean, msq = total[0:1], total[1:2]
    inv = lax.rsqrt(msq - mean * mean + 1e-05)
    cols = jnp.concatenate([mean, inv, jnp.zeros((6, toks), F32)], axis=0).T
    cgain = channel_gain[:, lanes]
    scaled = (cvt[...] - cols[:, 0:1]) * cols[:, 1:2] * cgain
    act[...] = (scaled * jax.nn.sigmoid(scaled)).astype(BF)

    def mixed_part(td):
        return dot_nt(glu[out_rows(td), 2 * chans:3 * chans], act[...])

    rs_first(0, mixed_part, pb, rb)
    rounds(late, 3, 4)
    rs_second(0, mixed_part, pb, rb, sb, cb)
    rounds(late, 4, 7)
    middle = (stream[...].astype(F32) + rs_third(0, sb, cb)).astype(BF)
    mid[...] = middle
    ag2[t] = middle.T
    ag_start(ag2, 1)
    rounds(late, 7, 9)
    ag_forward(ag2, 1, (1, 3))
    rounds(late, 9, 10)
    ag_forward(ag2, 1, (2,))
    rounds(late, 10, 11)
    ag_finish(ag2, 1)
    for b in range(3):
        normalize(ag2, ffn_gain, b)
        rounds(late, 11 + b, 12 + b)

    for d, n in ((CW, ncw), (CCW, nccw)):
        @pl.loop(1, n + 1)
        def _(s):
            ycopy(d, s, 1 - gi).wait_recv()

    ff = gu.shape[2]
    for b, lo in enumerate(range(0, ff, 256)):
        hi = min(lo + 256, ff)
        gate = dot_nn(nrm[...], gu[0, :, lo:hi])
        up = dot_nn(nrm[...], gu[1, :, lo:hi])
        hid[:, lo:hi] = (gate * jax.nn.sigmoid(gate) * up).astype(BF)
        if b < 2:
            rounds(late, 14 + b, 15 + b)
    rounds(late, 16, nz // 2 + 1)

    def ffn_part(td):
        return dot_nt(dn[out_rows(td), :], hid[...])

    rs_first(1, ffn_part, pb2, rb2)
    rs_second(1, ffn_part, pb2, rb2, sb2, cb2)

    for p in early + late:
        for d, n in ((CW, ncw), (CCW, nccw)):
            if p < 2:
                ref = glu.at[pl.ds(0, n * half), :]
            elif p < 6:
                ref = gu.at[0, pl.ds(0, n * quarter), :]
            else:
                ref = dn.at[pl.ds(0, n * quarter), :]
            pltpu.make_async_copy(ref, ref, zsend.at[d, p]).wait()
    ref = gu.at[0, pl.ds(0, (nz - 1) * srows), :]
    pltpu.make_async_copy(ref, ref, ysend).wait()
    ag_drain(ag1, 0)
    ag_drain(ag2, 1)
    for o in range(1, nt):
        st_copy(o, t, twin).wait_send()
    rs_drain(0, pb, rb, sb, cb)

    out[...] = (mid[...].astype(F32) + rs_third(1, sb2, cb2)).astype(BF)
    rs_drain(1, pb2, rb2, sb2, cb2)


def solution(mesh):
    nz, nt = mesh.shape["fs"], mesh.shape["tp"]

    def on_device(
        stream, mixer_gain, glu_value, glu_gate, conv_kernel, channel_gain,
        conv_out, ffn_gain, ffn_gate, ffn_up, ffn_down,
    ):
        rows, toks = stream.shape
        srows, chans = glu_value.shape
        ff = ffn_gate.shape[1]
        width = rows * nt
        nx = nt // 2
        vm = pl.BlockSpec(memory_space=pltpu.VMEM)
        hbm = pl.BlockSpec(memory_space=pl.ANY)
        dma = pltpu.SemaphoreType.DMA
        blocks = [
            pltpu.VMEM((nx, rows, toks), BF),
            pltpu.VMEM((nx, rows, toks), BF),
            pltpu.VMEM((nx - 1, rows, toks), BF),
            pltpu.VMEM((nx - 1, rows, toks), BF),
        ]
        return pl.pallas_call(
            functools.partial(kernel, nz, nt),
            out_shape=jax.ShapeDtypeStruct((rows, toks), BF),
            in_specs=[vm] * 5 + [hbm] * 6,
            out_specs=vm,
            scratch_shapes=[
                pltpu.VMEM((width, 3 * chans), BF),
                pltpu.VMEM((2, width, ff), BF),
                pltpu.VMEM((width, ff), BF),
                pltpu.VMEM((nt, toks, rows), BF),
                pltpu.VMEM((nt, toks, rows), BF),
                pltpu.VMEM((toks, width), BF),
                pltpu.VMEM((toks + 32, chans), F32),
                pltpu.VMEM((toks, chans), F32),
                pltpu.VMEM((toks, chans), BF),
                pltpu.VMEM((nt, 2, toks), F32),
                pltpu.VMEM((toks, ff), BF),
                pltpu.VMEM((rows, toks), F32),
                pltpu.VMEM((rows, toks), BF),
                *blocks, *blocks,
                dma((6,)),
                dma((2, 10)),
                dma((2, 10, nz // 2)),
                dma,
                dma((nz,)),
                dma((2, 4 + nx - 1)),
                dma((2, nt)),
                dma((nt,)),
                dma((nt,)),
                dma((2, nx)),
                dma((2, nx)),
                dma((2, nx - 1)),
                dma((2, nx - 1)),
            ],
            compiler_params=pltpu.CompilerParams(collective_id=0, has_side_effects=True),
        )(
            stream, mixer_gain[None, :], conv_kernel, channel_gain[None, :],
            ffn_gain[None, :], glu_value, glu_gate, conv_out, ffn_gate, ffn_up, ffn_down,
        )

    weight = P("fs", "tp")
    in_specs = (
        P("tp", ("grp", "fs")), P(), weight, weight, P(), P(), weight, P(),
        weight, weight, weight,
    )
    return jax.shard_map(
        on_device, mesh=mesh, in_specs=in_specs,
        out_specs=P("tp", ("grp", "fs")), check_vma=False,
    )
```

time: 481 us -> 178 us (0.37)
  waiting for transfers between devices: 273 us -> 0 us
  Pallas kernels: 0 us -> 176 us
  blocking collectives: 93.4 us -> 0 us
  starting transfers between devices: 70.3 us -> 0 us
  matrix products: 16.3 us -> 0 us
  between operations: 13.2 us -> 0.01 us
  other arithmetic: 9.04 us -> 0 us
    all_gather x3 -> x0, waiting for transfers between devices: 249 us -> none  [the longest x1 126 us: on_device(): down_whole = lax.all_gather(ffn_down, 'fs', axis=0, tiled=True)]
    pallas_call x0 -> x1, Pallas kernels: none -> 176 us  [on_device(): pl.pallas_call(functools.partial(kernel, nz, nt), out_shape=jax.ShapeDtyp...]
    all_to_all x3 -> x0, blocking collectives: 93.4 us -> none  [the longest x2 69.4 us: sent_and_summed(): lax.all_to_all(parts, axis, split_axis=0, concat_axis=0, tiled=True)]
    all_to_all x2 -> x0, starting transfers between devices: 70.3 us -> none  [copy_for_each(): lax.all_to_all(jnp.broadcast_to(value[None], (peers, *value.shape)), axis...]
    all_to_all x2 -> x0, waiting for transfers between devices: 23.1 us -> none  [copy_for_each(): lax.all_to_all(jnp.broadcast_to(value[None], (peers, *value.shape)), axis...]
    dot_general x5 -> x0, matrix products: 16.3 us -> none  [the longest x3 7.69 us: contract(): lax.dot_general(weight, acts, (((0,), (0,)), ((), ())), preferred_element...]
  transfers between devices with their start and end apart: 5 -> 0, of which waited for: 5 -> 0; matrix products, arithmetic and copies ran while one was open for 4% -> 0% of each run, Pallas kernels for 0% -> 0%
where the time goes in v1:
time: 178 us
  Pallas kernels  176 us (99%)
    pallas_call x1, Pallas kernels, on_device(): pl.pallas_call(functools.partial(kernel, nz, nt), out_shape=jax.ShapeDtyp...  176 us

profile of v1, /device:TPU:33, one launch (start us, length us, event | category | flops | bytes accessed | tf_op | source)
XLA Modules:
  0.0 178.0 jit_solution(16536193238930242096)
XLA Ops:
  0.0 176.4 %shard_map.109 = bf16[256,384]{1,0:T(8,128)(2,1)} custom-call(bf16[256,384]{1,0:T(8,128)(2,1)} %stream.1, f32[1,2048]{1,0:T(1,128)} %bitcast.3, bf16[31,1024]{1,0:T(8,128)(2,1)} %conv_kernel.1, f32[1,1024]{1,0:T(1,128)} %bitcast.5, f32[1,2048]{1,0:T(1,128)} %bitcast.4, bf16[64,128]{1,0:T(8,128)(2,1)} %gv.1, bf16[64,128]{1,0:T(8,128)(2,1)} %gg.1, ...), custom_call_target="tpu_custom_call" | custom-call | tf_op jit(solution)/shard_map/pallas_call | solution.py:374
  176.4 1.6 copy.13

commit v2 on v1

--- a/solution.py
+++ b/solution.py
@@ -10,6 +10,7 @@
 MESH = pl.DeviceIdType.MESH
 BF, F32 = jnp.bfloat16, jnp.float32
 CW, CCW = 0, 1
+PLACES = (0, 0, 0, 3, 3, 6, 18, 27, 28, 30, 31)
 
 
 def dot_nn(a, b):
@@ -24,9 +25,9 @@
     nz, nt,
     stream, mixer_gain, conv_kernel, channel_gain, ffn_gain, gv, gg, co, wg, wu, wd,
     out,
-    glu, gu, dn, ag1, ag2, nrm, pad, cvt, act, stats, hid, acc, mid,
+    glu, gu, dn, tail, ag1, ag2, nrm, pad, cvt, act, stats, hid, acc, mid,
     pb, rb, sb, cb, pb2, rb2, sb2, cb2,
-    loc_sem, zsend, zrecv, ysend, yrecv, ag_send, ag_recv, st_send, st_recv,
+    loc_sem, zsend, zrecv, ysend, yrecv, ytsend, ytrecv, ag_send, ag_recv, st_send, st_recv,
     d_send, d_recv, c_send, c_recv,
 ):
     g, z, t = lax.axis_index("grp"), lax.axis_index("fs"), lax.axis_index("tp")
@@ -48,16 +49,19 @@
         return lax.rem(x + o, nx) * 2 + core
 
     own = pl.ds(pl.multiple_of(z * srows, srows), srows)
+    main = gu.shape[2]
     locals_ = [
         pltpu.make_async_copy(gv, glu.at[own, pl.ds(0, chans)], loc_sem.at[0]),
         pltpu.make_async_copy(gg, glu.at[own, pl.ds(chans, chans)], loc_sem.at[1]),
         pltpu.make_async_copy(co, glu.at[own, pl.ds(2 * chans, chans)], loc_sem.at[2]),
-        pltpu.make_async_copy(wg, gu.at[0, own, :], loc_sem.at[3]),
-        pltpu.make_async_copy(wu, gu.at[1, own, :], loc_sem.at[4]),
-        pltpu.make_async_copy(wd, dn.at[own, :], loc_sem.at[5]),
+        pltpu.make_async_copy(wg.at[:, pl.ds(0, main)], gu.at[0, own, :], loc_sem.at[3]),
+        pltpu.make_async_copy(wu.at[:, pl.ds(0, main)], gu.at[1, own, :], loc_sem.at[4]),
+        pltpu.make_async_copy(wd.at[:, pl.ds(0, main)], dn.at[own, :], loc_sem.at[5]),
     ]
     for c in locals_:
         c.start()
+    for i, w in enumerate((wg, wu)):
+        tail[i, own, :] = jnp.concatenate([w[:, main:], wd[:, main:]], axis=1)
 
     barrier = pltpu.get_barrier_semaphore()
     for peer in (right, left):
@@ -67,7 +71,6 @@
         pl.semaphore_signal(
             barrier, inc=1, device_id={"tp": lax.rem(t + o, nt)}, device_id_type=MESH
         )
-    ag1[t] = stream[...].T
     for c in locals_:
         c.wait()
     pl.semaphore_wait(barrier, 2 + nt)
@@ -78,6 +81,8 @@
         base = zz * srows
         if p < 2:
             return glu.at[pl.ds(pl.multiple_of(base + half * p, half), half), :]
+        if p == 10:
+            return tail.at[gi, pl.ds(pl.multiple_of(base, srows), srows), :]
         k = (p - 2) % 4
         r = pl.ds(pl.multiple_of(base + quarter * k, quarter), quarter)
         return gu.at[gi, r, :] if p < 6 else dn.at[r, :]
@@ -101,6 +106,14 @@
         return pltpu.make_async_remote_copy(
             src_ref=gu.at[whose, r, :], dst_ref=gu.at[whose, r, :],
             send_sem=ysend, recv_sem=yrecv.at[i],
+            device_id={"grp": mate}, device_id_type=MESH,
+        )
+
+    def ytcopy(d, s, whose):
+        r = pl.ds(pl.multiple_of(held(d, s) * srows, srows), srows)
+        return pltpu.make_async_remote_copy(
+            src_ref=tail.at[whose, r, :], dst_ref=tail.at[whose, r, :],
+            send_sem=ytsend, recv_sem=ytrecv.at[d * ncw + s - 1],
             device_id={"grp": mate}, device_id_type=MESH,
         )
 
@@ -113,24 +126,44 @@
         if 5 in pieces:
             for d in dirs:
                 ycopy(d, s, gi).start()
+                ytcopy(d, s, gi).start()
+
+    glus, ms, ds = (0, 1), (2, 3, 4, 5, 10), (6, 7, 8, 9)
 
     def first(pieces):
         for p in pieces:
             for d in (CW, CCW):
                 send(p, d, 1)
 
-    def rounds(pieces, lo, hi):
-        top = min(hi, nccw)
-        if top > lo:
-            @pl.loop(lo, top)
-            def _(s):
-                step(pieces, s, (CW, CCW), (CW, CCW))
-        for s in range(max(lo, nccw), hi):
-            step(
-                pieces, s,
-                (CW, CCW) if s <= nccw else (CW,),
-                (CW,) if s < ncw else (),
-            )
+    def far_way(p):
+        return CCW if p in ds else CW
+
+    def whole(s, pieces):
+        step(pieces, s, (CW, CCW), (CW, CCW))
+
+    def last(s, pieces):
+        far = far_way(pieces[0])
+        dirs = (CW, CCW) if s <= nccw else (far,)
+        step(pieces, s, dirs, (far,) if s < ncw else ())
+
+    def any_step(s, pieces):
+        (whole if s < nccw else last)(s, pieces)
+
+    def unit(u):
+        if u <= ncw:
+            any_step(u, glus)
+        if u % 2:
+            any_step((u + 1) // 2, ms)
+        else:
+            any_step(u // 2, ds)
+
+    def units(lo, hi):
+        @pl.loop((lo + 1) // 2, (hi + 1) // 2)
+        def _(v):
+            whole(2 * v - 1, glus)
+            whole(v, ms)
+            whole(2 * v, glus)
+            whole(v, ds)
 
     def ag_copy(buf, which, block, k, target):
         return pltpu.make_async_remote_copy(
@@ -225,44 +258,30 @@
     def out_rows(td):
         return pl.ds(pl.multiple_of(td * rows, rows), rows)
 
-    early = (0, 1, 2, 3, 4, 5)
-    late = (6, 7, 8, 9)
-    first((0, 1))
+    first(glus)
+    first(ms)
+    first(ds)
+    ag1[t] = stream[...].T
     ag_start(ag1, 0)
-    first((2, 3, 4, 5))
-    rounds(early, 1, 4)
+    units(1, 5)
     ag_forward(ag1, 0, (1, 3))
-    rounds(early, 4, 5)
+    unit(5)
     ag_forward(ag1, 0, (2,))
-    rounds(early, 5, 7)
+    unit(6)
     ag_finish(ag1, 0)
     normalize(ag1, mixer_gain, 0)
-    rounds(early, 7, 8)
+    unit(7)
     normalize(ag1, mixer_gain, 1)
-    rounds(early, 8, 9)
+    unit(8)
     normalize(ag1, mixer_gain, 2)
     pad[0:32, :] = jnp.zeros((32, chans), F32)
-    rounds(early, 9, nz // 2)
-    first(late)
-    rounds(early, nz // 2, nz // 2 + 1)
-
-    both = dot_nn(nrm[...], glu[:, 0:2 * chans])
-    gated = both[:, :chans] * jax.nn.sigmoid(both[:, chans:])
-    pad[32:32 + toks, :] = gated.astype(BF).astype(F32)
-    rounds(late, 1, 2)
+    units(9, 15)
+    unit(15)
+    unit(16)
+
     lanes = pl.ds(pl.multiple_of(t * chans, chans), chans)
-    kern = conv_kernel[:, lanes].astype(F32)
     nb = 6
     bt = toks // nb
-    for b in range(nb):
-        total = jnp.zeros((bt, chans), F32)
-        for k in range(taps):
-            lo = b * bt + 32 - (taps - 1) + k
-            total = total + kern[k:k + 1, :] * pad[lo:lo + bt, :]
-        cvt[b * bt:(b + 1) * bt, :] = total
-    flipped = cvt[...].T
-    stats[t, 0:1, :] = jnp.sum(flipped, axis=0, keepdims=True)
-    stats[t, 1:2, :] = jnp.sum(flipped * flipped, axis=0, keepdims=True)
 
     def st_copy(o, src, target):
         return pltpu.make_async_remote_copy(
@@ -271,75 +290,114 @@
             device_id={"tp": target}, device_id_type=MESH,
         )
 
-    for o in range(1, nt):
-        st_copy(o, t, lax.rem(t + o, nt)).start()
-    rounds(late, 2, 3)
-    for o in range(1, nt):
-        st_copy(o, lax.rem(t + o, nt), lax.rem(t + o, nt)).wait_recv()
-    total = stats[0]
-    for j in range(1, nt):
-        total = total + stats[j]
-    total = total / (chans * nt)
-    mean, msq = total[0:1], total[1:2]
-    inv = lax.rsqrt(msq - mean * mean + 1e-05)
-    cols = jnp.concatenate([mean, inv, jnp.zeros((6, toks), F32)], axis=0).T
-    cgain = channel_gain[:, lanes]
-    scaled = (cvt[...] - cols[:, 0:1]) * cols[:, 1:2] * cgain
-    act[...] = (scaled * jax.nn.sigmoid(scaled)).astype(BF)
+    def gated():
+        both = dot_nn(nrm[...], glu[:, 0:2 * chans])
+        value = both[:, :chans] * jax.nn.sigmoid(both[:, chans:])
+        pad[32:32 + toks, :] = value.astype(BF).astype(F32)
+
+    def convolve(blocks):
+        kern = conv_kernel[:, lanes].astype(F32)
+        for b in blocks:
+            total = jnp.zeros((bt, chans), F32)
+            for k in range(taps):
+                lo = b * bt + 32 - (taps - 1) + k
+                total = total + kern[k:k + 1, :] * pad[lo:lo + bt, :]
+            cvt[b * bt:(b + 1) * bt, :] = total
+
+    def send_stats():
+        flipped = cvt[...].T
+        stats[t, 0:1, :] = jnp.sum(flipped, axis=0, keepdims=True)
+        stats[t, 1:2, :] = jnp.sum(flipped * flipped, axis=0, keepdims=True)
+        for o in range(1, nt):
+            st_copy(o, t, lax.rem(t + o, nt)).start()
 
     def mixed_part(td):
         return dot_nt(glu[out_rows(td), 2 * chans:3 * chans], act[...])
 
-    rs_first(0, mixed_part, pb, rb)
-    rounds(late, 3, 4)
-    rs_second(0, mixed_part, pb, rb, sb, cb)
-    rounds(late, 4, 7)
-    middle = (stream[...].astype(F32) + rs_third(0, sb, cb)).astype(BF)
-    mid[...] = middle
-    ag2[t] = middle.T
-    ag_start(ag2, 1)
-    rounds(late, 7, 9)
-    ag_forward(ag2, 1, (1, 3))
-    rounds(late, 9, 10)
-    ag_forward(ag2, 1, (2,))
-    rounds(late, 10, 11)
-    ag_finish(ag2, 1)
-    for b in range(3):
-        normalize(ag2, ffn_gain, b)
-        rounds(late, 11 + b, 12 + b)
-
-    for d, n in ((CW, ncw), (CCW, nccw)):
-        @pl.loop(1, n + 1)
-        def _(s):
-            ycopy(d, s, 1 - gi).wait_recv()
-
-    ff = gu.shape[2]
-    for b, lo in enumerate(range(0, ff, 256)):
-        hi = min(lo + 256, ff)
-        gate = dot_nn(nrm[...], gu[0, :, lo:hi])
-        up = dot_nn(nrm[...], gu[1, :, lo:hi])
-        hid[:, lo:hi] = (gate * jax.nn.sigmoid(gate) * up).astype(BF)
-        if b < 2:
-            rounds(late, 14 + b, 15 + b)
-    rounds(late, 16, nz // 2 + 1)
+    def activate():
+        for o in range(1, nt):
+            st_copy(o, lax.rem(t + o, nt), lax.rem(t + o, nt)).wait_recv()
+        total = stats[0]
+        for j in range(1, nt):
+            total = total + stats[j]
+        total = total / (chans * nt)
+        mean, msq = total[0:1], total[1:2]
+        inv = lax.rsqrt(msq - mean * mean + 1e-05)
+        cols = jnp.concatenate([mean, inv, jnp.zeros((6, toks), F32)], axis=0).T
+        scaled = (cvt[...] - cols[:, 0:1]) * cols[:, 1:2] * channel_gain[:, lanes]
+        act[...] = (scaled * jax.nn.sigmoid(scaled)).astype(BF)
+
+    def middle():
+        mid[...] = (stream[...].astype(F32) + rs_third(0, sb, cb)).astype(BF)
+        ag2[t] = mid[...].T
+        ag_start(ag2, 1)
+
+    def hand_over():
+        for d, n in ((CW, ncw), (CCW, nccw)):
+            @pl.loop(1, n + 1)
+            def _(s):
+                ycopy(d, s, 1 - gi).wait_recv()
+                ytcopy(d, s, 1 - gi).wait_recv()
+
+    def hide():
+        rest = tail.shape[2] // 2
+        for lo in range(0, main, 256):
+            hi = min(lo + 256, main)
+            gate = dot_nn(nrm[...], gu[0, :, lo:hi])
+            up = dot_nn(nrm[...], gu[1, :, lo:hi])
+            hid[:, lo:hi] = (gate * jax.nn.sigmoid(gate) * up).astype(BF)
+        gate, up = dot_nn(nrm[...], tail[0]), dot_nn(nrm[...], tail[1])
+        gate, up = gate[:, :rest], up[:, :rest]
+        ends = gate * jax.nn.sigmoid(gate) * up
+        hid[:, main:] = jnp.concatenate([jnp.zeros_like(ends), ends], axis=1).astype(BF)
+
+    events = (
+        gated,
+        lambda: convolve(range(nb // 2)),
+        lambda: [convolve(range(nb // 2, nb)), send_stats()],
+        activate,
+        lambda: rs_first(0, mixed_part, pb, rb),
+        lambda: rs_second(0, mixed_part, pb, rb, sb, cb),
+        middle,
+        lambda: ag_forward(ag2, 1, (1, 3)),
+        lambda: ag_forward(ag2, 1, (2,)),
+        lambda: ag_finish(ag2, 1),
+        lambda: [normalize(ag2, ffn_gain, b) for b in range(3)],
+    )
+    for k in range(2 * (nz - 16) + 1):
+        if k:
+            u = 16 + (k + 1) // 2
+            pieces = ms if u % 2 else ds
+            any_step((u + 1) // 2, pieces[:2] if k % 2 else pieces[2:])
+        for at, event in zip(PLACES, events):
+            if at == k:
+                event()
+    hand_over()
+    hide()
 
     def ffn_part(td):
-        return dot_nt(dn[out_rows(td), :], hid[...])
+        r = out_rows(td)
+        return dot_nt(dn[r, :], hid[:, :main]) + dot_nt(tail[0, r, :], hid[:, main:])
 
     rs_first(1, ffn_part, pb2, rb2)
     rs_second(1, ffn_part, pb2, rb2, sb2, cb2)
 
-    for p in early + late:
-        for d, n in ((CW, ncw), (CCW, nccw)):
+    for p in glus + ms + ds:
+        for d in (CW, CCW):
+            n = ncw if d == far_way(p) else nccw
             if p < 2:
                 ref = glu.at[pl.ds(0, n * half), :]
             elif p < 6:
                 ref = gu.at[0, pl.ds(0, n * quarter), :]
+            elif p < 10:
+                ref = dn.at[pl.ds(0, n * quarter), :]
             else:
-                ref = dn.at[pl.ds(0, n * quarter), :]
+                ref = tail.at[0, pl.ds(0, n * srows), :]
             pltpu.make_async_copy(ref, ref, zsend.at[d, p]).wait()
     ref = gu.at[0, pl.ds(0, (nz - 1) * srows), :]
     pltpu.make_async_copy(ref, ref, ysend).wait()
+    ref = tail.at[0, pl.ds(0, (nz - 1) * srows), :]
+    pltpu.make_async_copy(ref, ref, ytsend).wait()
     ag_drain(ag1, 0)
     ag_drain(ag2, 1)
     for o in range(1, nt):
@@ -360,6 +418,7 @@
         rows, toks = stream.shape
         srows, chans = glu_value.shape
         ff = ffn_gate.shape[1]
+        main = ff // 128 * 128
         width = rows * nt
         nx = nt // 2
         vm = pl.BlockSpec(memory_space=pltpu.VMEM)
@@ -374,12 +433,13 @@
         return pl.pallas_call(
             functools.partial(kernel, nz, nt),
             out_shape=jax.ShapeDtypeStruct((rows, toks), BF),
-            in_specs=[vm] * 5 + [hbm] * 6,
+            in_specs=[vm] * 5 + [hbm] * 3 + [vm] * 3,
             out_specs=vm,
             scratch_shapes=[
                 pltpu.VMEM((width, 3 * chans), BF),
-                pltpu.VMEM((2, width, ff), BF),
-                pltpu.VMEM((width, ff), BF),
+                pltpu.VMEM((2, width, main), BF),
+                pltpu.VMEM((width, main), BF),
+                pltpu.VMEM((2, width, 2 * (ff - main)), BF),
                 pltpu.VMEM((nt, toks, rows), BF),
                 pltpu.VMEM((nt, toks, rows), BF),
                 pltpu.VMEM((toks, width), BF),
@@ -387,13 +447,15 @@
                 pltpu.VMEM((toks, chans), F32),
                 pltpu.VMEM((toks, chans), BF),
                 pltpu.VMEM((nt, 2, toks), F32),
-                pltpu.VMEM((toks, ff), BF),
+                pltpu.VMEM((toks, main + 2 * (ff - main)), BF),
                 pltpu.VMEM((rows, toks), F32),
                 pltpu.VMEM((rows, toks), BF),
                 *blocks, *blocks,
                 dma((6,)),
-                dma((2, 10)),
-                dma((2, 10, nz // 2)),
+                dma((2, 11)),
+                dma((2, 11, nz // 2)),
+                dma,
+                dma((nz,)),
                 dma,
                 dma((nz,)),
                 dma((2, 4 + nx - 1)),

time: 178 us -> 164 us (0.921)
  Pallas kernels: 176 us -> 162 us
    pallas_call x1, Pallas kernels: 176 us -> 162 us  [on_device(): pl.pallas_call(functools.partial(kernel, nz, nt), out_shape=jax.ShapeDtyp...]
where the time goes in v2:
time: 164 us
  Pallas kernels  162 us (99%)
    pallas_call x1, Pallas kernels, on_device(): pl.pallas_call(functools.partial(kernel, nz, nt), out_shape=jax.ShapeDtyp...  162 us

profile of v2, /device:TPU:33, one launch (start us, length us, event | category | flops | bytes accessed | tf_op | source)
XLA Modules:
  0.0 163.6 jit_solution(11638094815069637932)
XLA Ops:
  0.0 162.0 %shard_map.109 = bf16[256,384]{1,0:T(8,128)(2,1)} custom-call(bf16[256,384]{1,0:T(8,128)(2,1)} %stream.1, f32[1,2048]{1,0:T(1,128)} %bitcast.3, bf16[31,1024]{1,0:T(8,128)(2,1)} %conv_kernel.1, f32[1,1024]{1,0:T(1,128)} %bitcast.5, f32[1,2048]{1,0:T(1,128)} %bitcast.4, bf16[64,128]{1,0:T(8,128)(2,1)} %gv.1, bf16[64,128]{1,0:T(8,128)(2,1)} %gg.1, ...), custom_call_target="tpu_custom_call" | custom-call | tf_op jit(solution)/shard_map/pallas_call | solution.py:433
  162.0 1.6 copy.13

commit v3 on v2

--- a/solution.py
+++ b/solution.py
@@ -10,7 +10,8 @@
 MESH = pl.DeviceIdType.MESH
 BF, F32 = jnp.bfloat16, jnp.float32
 CW, CCW = 0, 1
-PLACES = (0, 0, 0, 3, 3, 6, 18, 27, 28, 30, 31)
+PLACES = (0, 0, 0, 3, 3, 6, 18, 27, 28, 29, 30, 30, 30)
+LEAD = 1
 
 
 def dot_nn(a, b):
@@ -48,6 +49,14 @@
     def at_chip(o):
         return lax.rem(x + o, nx) * 2 + core
 
+    barrier = pltpu.get_barrier_semaphore()
+    for peer in (right, left):
+        pl.semaphore_signal(barrier, inc=1, device_id={"fs": peer}, device_id_type=MESH)
+    pl.semaphore_signal(barrier, inc=1, device_id={"grp": mate}, device_id_type=MESH)
+    for o in range(1, nt):
+        pl.semaphore_signal(
+            barrier, inc=1, device_id={"tp": lax.rem(t + o, nt)}, device_id_type=MESH
+        )
     own = pl.ds(pl.multiple_of(z * srows, srows), srows)
     main = gu.shape[2]
     locals_ = [
@@ -60,18 +69,7 @@
     ]
     for c in locals_:
         c.start()
-    for i, w in enumerate((wg, wu)):
-        tail[i, own, :] = jnp.concatenate([w[:, main:], wd[:, main:]], axis=1)
-
-    barrier = pltpu.get_barrier_semaphore()
-    for peer in (right, left):
-        pl.semaphore_signal(barrier, inc=1, device_id={"fs": peer}, device_id_type=MESH)
-    pl.semaphore_signal(barrier, inc=1, device_id={"grp": mate}, device_id_type=MESH)
-    for o in range(1, nt):
-        pl.semaphore_signal(
-            barrier, inc=1, device_id={"tp": lax.rem(t + o, nt)}, device_id_type=MESH
-        )
-    for c in locals_:
+    for c in locals_[:3]:
         c.wait()
     pl.semaphore_wait(barrier, 2 + nt)
 
@@ -259,6 +257,11 @@
         return pl.ds(pl.multiple_of(td * rows, rows), rows)
 
     first(glus)
+    for i, w in enumerate((wg, wu)):
+        tail[i, own, :] = jnp.concatenate([w[:, main:], wd[:, main:]], axis=1)
+
+    for c in locals_[3:]:
+        c.wait()
     first(ms)
     first(ds)
     ag1[t] = stream[...].T
@@ -363,17 +366,22 @@
         lambda: ag_forward(ag2, 1, (2,)),
         lambda: ag_finish(ag2, 1),
         lambda: [normalize(ag2, ffn_gain, b) for b in range(3)],
+        hand_over,
+        hide,
     )
-    for k in range(2 * (nz - 16) + 1):
+    mid_step = ncw // 2 + 1
+    rest_steps = [(ms, s) for s in range(mid_step, mid_step + LEAD)]
+    for s in range(mid_step, ncw + 1):
+        if s + LEAD <= ncw:
+            rest_steps.append((ms, s + LEAD))
+        rest_steps.append((ds, s))
+    for k in range(2 * len(rest_steps) + 1):
         if k:
-            u = 16 + (k + 1) // 2
-            pieces = ms if u % 2 else ds
-            any_step((u + 1) // 2, pieces[:2] if k % 2 else pieces[2:])
+            pieces, s = rest_steps[(k - 1) // 2]
+            any_step(s, pieces[:2] if k % 2 else pieces[2:])
         for at, event in zip(PLACES, events):
             if at == k:
                 event()
-    hand_over()
-    hide()
 
     def ffn_part(td):
         r = out_rows(td)

time: 164 us -> 163 us (level)
  no operation moved by 1% of the time
where the time goes in v3:
time: 163 us
  Pallas kernels  161 us (99%)
    pallas_call x1, Pallas kernels, on_device(): pl.pallas_call(functools.partial(kernel, nz, nt), out_shape=jax.ShapeDtyp...  161 us

profile of v3, /device:TPU:33, one launch (start us, length us, event | category | flops | bytes accessed | tf_op | source)
XLA Modules:
  0.0 163.1 jit_solution(17370454671276601152)
XLA Ops:
  0.0 161.5 %shard_map.109 = bf16[256,384]{1,0:T(8,128)(2,1)} custom-call(bf16[256,384]{1,0:T(8,128)(2,1)} %stream.1, f32[1,2048]{1,0:T(1,128)} %bitcast.3, bf16[31,1024]{1,0:T(8,128)(2,1)} %conv_kernel.1, f32[1,1024]{1,0:T(1,128)} %bitcast.5, f32[1,2048]{1,0:T(1,128)} %bitcast.4, bf16[64,128]{1,0:T(8,128)(2,1)} %gv.1, bf16[64,128]{1,0:T(8,128)(2,1)} %gg.1, ...), custom_call_target="tpu_custom_call" | custom-call | tf_op jit(solution)/shard_map/pallas_call | solution.py:441
  161.5 1.6 copy.13
